TPU v7x, 32 devices: a whole 2x2x4 slice. The times are simulated.
32 devices in a mesh: sp: 16 (over z, y, x), tp: 2 (over core).
Axes of the slice: x: 2, y: 2, z: 4, core: 2. Of those that a mesh axis runs over, the one named last changes fastest.
Arguments:
- tokens: bfloat16 [6144, 2048], P('sp', 'tp'), may hold values from -6 to 6
- input_gain: float32 [2048], replicated, may hold values from 0.1 to 1.9
- query_weight: bfloat16 [2048, 1024], P(None, 'tp'), may hold values from -0.5 to 0.5
- query_rot_weight: bfloat16 [2048, 512], P(None, 'tp'), may hold values from -0.125 to 0.125
- kv_down: bfloat16 [2048, 256], replicated, may hold values from -0.5 to 0.5
- rot_down: bfloat16 [2048, 32], replicated, may hold values from -0.125 to 0.125
- kv_gain: float32 [256], replicated, may hold values from 0.1 to 1.9
- key_up: bfloat16 [256, 1024], P(None, 'tp'), may hold values from -0.5 to 0.5
- value_up: bfloat16 [256, 1024], P(None, 'tp'), may hold values from -4 to 4
- conv_value_weight: bfloat16 [2048, 1024], P(None, 'tp'), may hold values from -0.125 to 0.125
- conv_gate_weight: bfloat16 [2048, 1024], P(None, 'tp'), may hold values from -0.125 to 0.125
- conv_taps: float32 [31, 1024], P(None, 'tp'), may hold values from -8 to 8
- conv_ln_gain: float32 [1024], P('tp'), may hold values from 0.1 to 1.9
- conv_ln_bias: float32 [1024], P('tp'), may hold values from -3 to 3
- att_out_gain: float32 [1024], P('tp'), may hold values from 0.1 to 1.9
- conv_out_gain: float32 [1024], P('tp'), may hold values from 0.1 to 1.9
- att_out_weight: bfloat16 [1024, 2048], P('tp'), may hold values from -0.125 to 0.125
- conv_out_weight: bfloat16 [1024, 2048], P('tp'), may hold values from -0.125 to 0.125
Outputs:
- mixed: bfloat16 [6144, 2048], P('sp', 'tp')
All inputs are finite; a program needn't handle non-finite values.
Results may differ from a plain program's by a relative error of at most 0.017.
Values may be sent and summed in bfloat16 or wider, within the bound.
No kernel may reach another device: no remote copies, remote signals or barrier semaphores. Data moves between devices by JAX's collectives and lax.ppermute only.
A program may use at most 128 MiB of HBM per device.

v0:
```python
import math
import jax
import jax.numpy as jnp
from jax import lax
from jax.sharding import PartitionSpec as P

D_MODEL = 2048
NOPE_DIM = 64
ROT_DIM = 32
VALUE_DIM = 64
CONV_CH = 1024
KERNEL = 31
ATT_WIDTH = 1024
norm_eps = 1e-06
far_below = -1e30
rope_base = 10000.0


def shifted(block, axis, distance):
    devices = range(lax.axis_size(axis))
    route = [(i - distance, i) for i in devices if i - distance in devices]
    return lax.ppermute(block, axis, route)


def rotary_tables(positions, half_dim):
    frequency = rope_base ** (-jnp.arange(half_dim, dtype=jnp.float32) / half_dim)
    angles = positions.astype(jnp.float32)[:, None] * frequency[None, :]
    return (jnp.cos(angles), jnp.sin(angles))


def rotate_half(values, cos_table, sine_table):
    half_dim = cos_table.shape[-1]
    front_half = values[..., :half_dim]
    back_half = values[..., half_dim:]
    return jnp.concatenate(
        [
            front_half * cos_table - back_half * sine_table,
            back_half * cos_table + front_half * sine_table,
        ],
        axis=-1,
    )


def shards(
    tokens,
    input_gain,
    query_weight,
    query_rot_weight,
    kv_down,
    rot_down,
    kv_gain,
    key_up,
    value_up,
    conv_value_weight,
    conv_gate_weight,
    conv_taps,
    conv_ln_gain,
    conv_ln_bias,
    att_out_gain,
    conv_out_gain,
    att_out_weight,
    conv_out_weight,
):
    tok_rows = tokens.shape[0]
    heads_here = key_up.shape[1] // NOPE_DIM
    chan_here = conv_taps.shape[1]
    weight_list = (
        query_weight,
        query_rot_weight,
        kv_down,
        rot_down,
        conv_value_weight,
        conv_gate_weight,
    )
    wide_part = lax.all_gather(tokens, "tp", axis=1, tiled=True).astype(jnp.float32)
    scaled = (wide_part * input_gain[None, :]).astype(jnp.bfloat16)

    def add_product(weight):
        return jnp.dot(scaled, weight, preferred_element_type=jnp.float32)

    summed = tuple((add_product(weight) for weight in weight_list))
    q_acc, qrot_acc, latent_raw, rot_acc, value_acc, gate_acc, square_sum = summed + (
        jnp.sum(wide_part * wide_part, axis=1),
    )
    row_scale = lax.rsqrt(square_sum / D_MODEL + norm_eps)[:, None]
    positions = lax.axis_index("sp") * tok_rows + jnp.arange(tok_rows, dtype=jnp.int32)
    cos_table, sine_table = rotary_tables(positions, ROT_DIM // 2)
    queries = (q_acc * row_scale).astype(jnp.bfloat16).reshape(tok_rows, heads_here, NOPE_DIM)
    query_rot = rotate_half(
        (qrot_acc * row_scale).reshape(tok_rows, heads_here, ROT_DIM),
        cos_table[:, None, :],
        sine_table[:, None, :],
    ).astype(jnp.bfloat16)
    latent = (
        latent_raw
        * lax.rsqrt(jnp.mean(latent_raw * latent_raw, axis=1, keepdims=True) + norm_eps)
        * kv_gain[None, :]
    ).astype(jnp.bfloat16)
    key_rot = rotate_half(rot_acc * row_scale, cos_table, sine_table).astype(jnp.bfloat16)
    gated_input = (value_acc * row_scale * jax.nn.sigmoid(gate_acc * row_scale)).astype(
        jnp.bfloat16
    )
    query_end = (lax.axis_index("sp") + 1) * tok_rows
    inv_scale = 1.0 / math.sqrt(NOPE_DIM + ROT_DIM)

    def attend(carried, key_block, rot_block, value_block, key_offset):
        run_max, run_sum, run_acc = carried
        block_len = key_block.shape[0]
        scores = (
            jnp.einsum("qhd,khd->hqk", queries, key_block, preferred_element_type=jnp.float32)
            + jnp.einsum("qhd,kd->hqk", query_rot, rot_block, preferred_element_type=jnp.float32)
        ) * inv_scale
        key_pos = key_offset + jnp.arange(block_len, dtype=jnp.int32)
        visible = (key_pos[None, :] <= positions[:, None])[None]
        new_max = jnp.maximum(run_max, jnp.max(jnp.where(visible, scores, far_below), axis=2))
        exp_scores = jnp.where(visible, jnp.exp(scores - new_max[:, :, None]), 0.0)
        shrink = jnp.exp(run_max - new_max)
        run_sum = run_sum * shrink + jnp.sum(exp_scores, axis=2)
        run_acc = run_acc * shrink.T[:, :, None] + jnp.einsum(
            "hqk,khd->qhd",
            exp_scores.astype(jnp.bfloat16),
            value_block,
            preferred_element_type=jnp.float32,
        )
        return (new_max, run_sum, run_acc)

    def expand_latent(sliced):
        lat_block, rot_block = sliced
        key_block = (
            jnp.dot(lat_block, key_up, preferred_element_type=jnp.float32)
            .astype(jnp.bfloat16)
            .reshape(-1, heads_here, NOPE_DIM)
        )
        value_block = (
            jnp.dot(lat_block, value_up, preferred_element_type=jnp.float32)
            .astype(jnp.bfloat16)
            .reshape(-1, heads_here, VALUE_DIM)
        )
        return (key_block, value_block, rot_block)

    def square_rows(matrix):
        wide_rows = matrix.astype(jnp.float32)
        return jnp.sum(wide_rows * wide_rows, axis=1)

    start_state = (
        jnp.full((heads_here, tok_rows), far_below, jnp.float32),
        jnp.zeros((heads_here, tok_rows), jnp.float32),
        jnp.zeros((tok_rows, heads_here, VALUE_DIM), jnp.float32),
    )
    pieces = (
        lax.all_gather(latent, "sp", axis=0, tiled=True),
        lax.all_gather(key_rot, "sp", axis=0, tiled=True),
    )
    piece_rows = pieces[0].shape[0]
    step_len = math.gcd(piece_rows, 512)

    def visit_block(running, block_idx):
        start_row = block_idx * step_len
        sliced = tuple(
            (lax.dynamic_slice_in_dim(member, start_row, step_len, 0) for member in pieces)
        )

        def compute(current):
            key_block, value_block, rot_block = expand_latent(sliced)
            return attend(current, key_block, rot_block, value_block, start_row)

        return (lax.cond(start_row < query_end, compute, lambda current: current, running), None)

    final_state = lax.scan(
        visit_block, start_state, jnp.arange(piece_rows // step_len, dtype=jnp.int32)
    )[0]
    run_max, run_sum, run_acc = final_state
    attended = (
        (run_acc / run_sum.T[:, :, None])
        .astype(jnp.bfloat16)
        .reshape(tok_rows, heads_here * VALUE_DIM)
    )
    att_sq = lax.psum(square_rows(attended), "tp")
    rim_rows = shifted(gated_input[tok_rows - (KERNEL - 1) :], "sp", 1)
    padded = jnp.concatenate([rim_rows, gated_input], axis=0)
    conv_out = jnp.zeros((tok_rows, chan_here), jnp.float32)
    for tap_idx in range(KERNEL):
        conv_out = conv_out + conv_taps[tap_idx][None, :] * padded[
            tap_idx : tap_idx + tok_rows
        ].astype(jnp.float32)
    moment_one, moment_two = lax.psum(
        (jnp.sum(conv_out, axis=1), jnp.sum(conv_out * conv_out, axis=1)), "tp"
    )
    mean_val = moment_one / CONV_CH
    spread = moment_two / CONV_CH - mean_val * mean_val
    normed = (conv_out - mean_val[:, None]) * lax.rsqrt(spread + norm_eps)[:, None]
    swished = jax.nn.silu(normed * conv_ln_gain[None, :] + conv_ln_bias[None, :])
    conv_sq = lax.psum(square_rows(swished), "tp")
    att_mixed = (
        attended.astype(jnp.float32)
        * lax.rsqrt(att_sq / ATT_WIDTH + norm_eps)[:, None]
        * att_out_gain[None, :]
    ).astype(jnp.bfloat16)
    conv_mixed = (
        swished * lax.rsqrt(conv_sq / CONV_CH + norm_eps)[:, None] * conv_out_gain[None, :]
    ).astype(jnp.bfloat16)
    contract = (((0,), (1,)), ((), ()))
    feature_rows = lax.psum_scatter(
        (
            lax.dot_general(att_out_weight, att_mixed, contract, preferred_element_type=jnp.float32)
            + lax.dot_general(
                conv_out_weight, conv_mixed, contract, preferred_element_type=jnp.float32
            )
        ).astype(jnp.bfloat16),
        "tp",
        scatter_dimension=0,
        tiled=True,
    ).astype(jnp.float32)
    return feature_rows.T.astype(jnp.bfloat16)


def solution(mesh):
    return jax.shard_map(
        shards,
        mesh=mesh,
        in_specs=(
            P("sp", "tp"),
            P(),
            P(None, "tp"),
            P(None, "tp"),
            P(),
            P(),
            P(),
            P(None, "tp"),
            P(None, "tp"),
            P(None, "tp"),
            P(None, "tp"),
            P(None, "tp"),
            P("tp"),
            P("tp"),
            P("tp"),
            P("tp"),
            P("tp", None),
            P("tp", None),
        ),
        out_specs=P("sp", "tp"),
        check_vma=False,
    )
```

profile of v0, /device:TPU:0, one launch (start us, length us, event | category | flops | bytes accessed | tf_op | source)
XLA Modules:
  0.0 248.4 jit_solution(14839390345446647439)
XLA Ops:
  7.3 14.1 %all-gather.3.cloned.1.call-done = bf16[384,2048]{1,0:T(8,128)(2,1)} async-done(((bf16[384,1024]{1,0:T(8,128)(2,1)}), bf16[384,2048]{1,0:T(8,128)(2,1)}) %all-gather.3.cloned.1.call-update) | async-done | bytes 1572880 | tf_op jit(solution)/shard_map/all_gather | solution.py:75
  21.4 2.5 multiply_reduce_fusion.3
  25.6 1.8 fusion.27
  27.4 3.3 %fusion.33 = f32[384,512]{1,0:T(8,128)S(1)} fusion(bf16[2048,512]{1,0:T(8,128)(2,1)} %param.32, bf16[384,2048]{1,0:T(8,128)(2,1)} %all-gather.3.cloned.1.call-done, f32[2048]{0:T(1024)S(1)} %copy-done.16, f32[384]{0:T(512)S(1)} %add_rsqrt_fusion.3), kind=kOutput, calls=%fused_computation.72 | convolution fusion | flops 808452096 | bytes 4466176 | tf_op jit(solution)/shard_map/dot_general | solution.py:79
  30.8 1.0 fusion.35
  31.8 3.8 %collective-permute-start = (bf16[30,512]{1,0:T(8,128)(2,1)S(1)}, bf16[30,512]{1,0:T(8,128)(2,1)S(1)}, u32[]{:S(2)}, u32[]{:S(2)}) collective-permute-start(bf16[30,512]{1,0:T(8,128)(2,1)S(1)} %slice.268), channel_id=1, source_target_pairs={{0,2},{2,4},{4,6},{6,8},{8,10},{10,12},{12,14},{14,16},{16,18},{18... | collective-permute-start | bytes 92168 | tf_op jit(solution)/shard_map/ppermute | solution.py:22
  36.4 44.6 %all_gather.11 = bf16[6144,32]{0,1:T(8,128)(2,1)} all-gather(bf16[384,32]{0,1:T(8,128)(2,1)S(1)} %pad_maximum_fusion.2), channel_id=1, replica_groups=mesh['sp'=16,'tp'=2] {'sp'}, dimensions={0}, use_global_device_ids=true | all-gather | bytes 417792 | tf_op jit(solution)/shard_map/all_gather | solution.py:152
  83.0 14.7 %fusion.77 = (f32[384]{0:T(512)}, f32[384]{0:T(512)}, f32[384,512]{1,0:T(8,128)S(1)}) fusion(bf16[384,512]{1,0:T(8,128)(2,1)} %copy-done.5, f32[512]{0:T(512)S(1)} %bitcast.93, bf16[30,512]{1,0:T(8,128)(2,1)S(1)} %collective-permute-done, f32[512]{0:T(512)S(1)} %bitcast.94, f32[512]{0:T(512)} %bitcast.96, f32[512]{0:T(512)} %bitcast.97, f32[512]{0:T(512)} %bitcast.98, ...), kind=kLoop, calls=%fused_computation.145 | loop fusion | flops 36371712 | bytes 1276928 | tf_op jit(solution)/shard_map/reduce_sum | solution.py:187
  97.7 2.8 %all-reduce.1 = (f32[384]{0:T(512)S(1)}, f32[384]{0:T(512)S(1)}) all-reduce(f32[384]{0:T(512)} %get-tuple-element.271, f32[384]{0:T(512)} %get-tuple-element.270), channel_id=1, replica_groups=mesh['sp'=16,'tp'=2] {'tp'}, use_global_device_ids=true, to_apply=%region_13.14 | all-reduce | flops 768 | bytes 6144 | tf_op jit(solution)/shard_map/psum | solution.py:186
  100.5 1.2 multiply_reduce_fusion
  101.7 4.7 %copy.24 = bf16[6144,256]{1,0:T(8,128)(2,1)} copy(bf16[6144,256]{0,1:T(8,128)(2,1)} %all-gather.5.cloned.1.call-done) | data formatting | bytes 6291456
  106.4 24.4 %while.15 = (s32[]{:T(128)}, f32[8,384]{1,0:T(8,128)S(1)}, f32[8,384]{1,0:T(8,128)S(1)}, f32[384,8,64]{0,2,1:T(8,128)S(1)}, s32[12]{0:T(128)S(1)}, /*index=5*/s3...) while((s32[]{:T(128)}, f32[8,384]{1,0:T(8,128)S(1)}, ...), condition=%wide.region_7.8_spmd.clone, body=%wide.region_2.7_spmd.clone.sunk | while | flops 788604800 | bytes 38840728 | solution.py:169
  107.7 9.0 %conditional.3 = ((f32[8,384]{1,0:T(8,128)S(1)}, f32[8,384]{1,0:T(8,128)S(1)}, f32[384,8,64]{0,2,1:T(8,128)S(1)})) conditional(s32[]{:T(128)} %convert_element_type.326, (f32[8,384]{1,0:T(8,128)S(1)}, f32[8,384]{1,0:T(8,128)S(1)}, f32[384,8,64]{0,2,1:T(8,128)S(1)}) %tuple.85, (s32[]{:T(128)}, s32[]{:T(128)}, bf16[6144,256]{1,0:T(8,128)(2,1)}, ...), branch_computations={%region_3.3_spmd, %region_4.6_spmd} | conditional | flops 788604800 | bytes 38838896 | solution.py:167
  107.7 1.4 convolution_convert_fusion.1
  109.1 1.9 fusion.18
  111.2 1.6 select_reduce_fusion
  112.8 1.3 convolution_convert_fusion
  114.1 1.4 fusion.13
  115.5 1.1 fusion.4
  131.8 2.4 all-reduce
  134.3 1.4 fusion.37
  135.8 1.0 fusion.81
  136.8 2.5 fusion.28
  139.3 102.5 %reduce-scatter.2.cloned.1.call-done = bf16[1024,384]{0,1:T(8,128)(2,1)} async-done(((bf16[2048,384]{0,1:T(8,128)(2,1)}), bf16[1024,384]{0,1:T(8,128)(2,1)}) %reduce-scatter.2.cloned.1.call-update) | async-done | bytes 786448 | tf_op jit(solution)/shard_map/reduce_scatter | solution.py:203
  (108 shorter events, 13.7 us)
Async XLA Ops:
  6.5 129.2 %copy-start = (bf16[512,2048]{1,0:T(8,128)(2,1)S(1)}, bf16[512,2048]{1,0:T(8,128)(2,1)}, u32[]{:S(2)}) copy-start(bf16[512,2048]{1,0:T(8,128)(2,1)} %param.38) | copy-start | bytes 6291460
  6.5 17.4 %copy-start.10 = (f32[256]{0:T(256)S(1)}, f32[256]{0:T(256)}, u32[]{:S(2)}) copy-start(f32[256]{0:T(256)} %param.28) | copy-start | bytes 3076
  6.5 18.3 %copy-start.6 = (f32[31,512]{1,0:T(8,128)S(1)}, f32[31,512]{1,0:T(8,128)}, u32[]{:S(2)}) copy-start(f32[31,512]{1,0:T(8,128)} %param.33) | copy-start | bytes 190468
  6.5 14.9 %all-gather.3.cloned.1.call-start = ((), (), s32[]{:S(2)}) async-start(), calls=%async_computation.1 | async-start | bytes 2359296 | tf_op jit(solution)/shard_map/all_gather | solution.py:75
  7.3 20.1 %copy-start.16 = (f32[2048]{0:T(1024)S(1)}, f32[2048]{0:T(1024)}, u32[]{:S(2)}) copy-start(f32[2048]{0:T(1024)} %param.23) | copy-start | bytes 24580
  7.3 94.4 %all-gather.5.cloned.1.call-start = ((), (), s32[]{:S(2)}) async-start(), calls=%async_computation.2 | async-start | bytes 3342336 | tf_op jit(solution)/shard_map/all_gather | solution.py:151
  24.8 217.1 %reduce-scatter.2.cloned.1.call-start = ((), (), s32[]{:S(2)}) async-start(), calls=%async_computation.3 | async-start | bytes 2359296 | tf_op jit(solution)/shard_map/reduce_scatter | solution.py:203
  27.4 3.4 %copy-start.4 = (bf16[384,2048]{1,0:T(8,128)(2,1)S(1)}, bf16[384,2048]{1,0:T(8,128)(2,1)}, u32[]{:S(2)}) copy-start(bf16[384,2048]{1,0:T(8,128)(2,1)} %all-gather.3.cloned.1.call-done) | copy-start | bytes 4718596
  27.4 3.4 %copy-start.11 = (bf16[2048,512]{1,0:T(8,128)(2,1)S(1)}, bf16[2048,512]{1,0:T(8,128)(2,1)}, u32[]{:S(2)}) copy-start(bf16[2048,512]{1,0:T(8,128)(2,1)} %param.31) | copy-start | bytes 6291460
  30.7 4.8 %copy-start.15 = (bf16[2048,32]{0,1:T(8,128)(2,1)S(1)}, bf16[2048,32]{0,1:T(8,128)(2,1)}, u32[]{:S(2)}) copy-start(bf16[2048,32]{0,1:T(8,128)(2,1)} %param.27) | copy-start | bytes 393220
  30.8 50.2 %copy-start.14 = (bf16[2048,256]{1,0:T(8,128)(2,1)S(1)}, bf16[2048,256]{1,0:T(8,128)(2,1)}, u32[]{:S(2)}) copy-start(bf16[2048,256]{1,0:T(8,128)(2,1)} %param.25) | copy-start | bytes 3145732
  31.8 50.0 %copy-start.5 = (bf16[384,512]{1,0:T(8,128)(2,1)}, bf16[384,512]{1,0:T(8,128)(2,1)S(1)}, u32[]{:S(2)}) copy-start(bf16[384,512]{1,0:T(8,128)(2,1)S(1)} %fusion.35) | copy-start | bytes 1179652
  31.8 50.0 %copy-start.12 = (bf16[2048,512]{1,0:T(8,128)(2,1)S(1)}, bf16[2048,512]{1,0:T(8,128)(2,1)}, u32[]{:S(2)}) copy-start(bf16[2048,512]{1,0:T(8,128)(2,1)} %param.24) | copy-start | bytes 6291460
  31.8 51.2 %collective-permute-start = (bf16[30,512]{1,0:T(8,128)(2,1)S(1)}, bf16[30,512]{1,0:T(8,128)(2,1)S(1)}, u32[]{:S(2)}, u32[]{:S(2)}) collective-permute-start(bf16[30,512]{1,0:T(8,128)(2,1)S(1)} %slice.268), channel_id=1, source_target_pairs={{0,2},{2,4},{4,6},{6,8},{8,10},{10,12},{12,14},{14,16},{16,18},{18... | collective-permute-start | bytes 92168 | tf_op jit(solution)/shard_map/ppermute | solution.py:22
  97.7 8.6 %copy-start.2 = (f32[384,512]{1,0:T(8,128)}, f32[384,512]{1,0:T(8,128)S(1)}, u32[]{:S(2)}) copy-start(f32[384,512]{1,0:T(8,128)S(1)} %get-tuple-element.304) | copy-start | bytes 2359300
  106.4 27.9 %copy-start.7 = (f32[512]{0:T(512)S(1)}, f32[512]{0:T(512)}, u32[]{:S(2)}) copy-start(f32[512]{0:T(512)} %param.36) | copy-start | bytes 6148
  111.2 1.6 copy-start.1
  134.3 2.5 %copy-start.3 = (f32[384,512]{1,0:T(8,128)S(1)}, f32[384,512]{1,0:T(8,128)}, u32[]{:S(2)}) copy-start(f32[384,512]{1,0:T(8,128)} %copy-done.2) | copy-start | bytes 2359300
  134.3 2.5 %copy-start.8 = (f32[512]{0:T(512)S(1)}, f32[512]{0:T(512)}, u32[]{:S(2)}) copy-start(f32[512]{0:T(512)} %param.35) | copy-start | bytes 6148
  134.3 2.5 %copy-start.9 = (f32[512]{0:T(512)S(1)}, f32[512]{0:T(512)}, u32[]{:S(2)}) copy-start(f32[512]{0:T(512)} %param.34) | copy-start | bytes 6148
  134.3 2.5 %copy-start.13 = (bf16[512,2048]{1,0:T(8,128)(2,1)S(1)}, bf16[512,2048]{1,0:T(8,128)(2,1)}, u32[]{:S(2)}) copy-start(bf16[512,2048]{1,0:T(8,128)(2,1)} %param.39) | copy-start | bytes 6291460
  134.3 2.5 %copy-start.17 = (f32[512]{0:T(512)S(1)}, f32[512]{0:T(512)}, u32[]{:S(2)}) copy-start(f32[512]{0:T(512)} %param.37) | copy-start | bytes 6148
Sparse Core Ops, SparseCore 0:
  8.9 12.5 all-gather.2
  24.9 72.0 all-gather.4
  139.5 102.3 reduce-scatter.1
where the time goes:
time: 250 us; the launch traced here: 248 us
  waiting for transfers between devices  117 us (47%)
  blocking collectives  49.8 us (20%)
  other arithmetic  22.4 us (9%)
  matrix products  20.1 us (8%)
  between operations  13.5 us (5%)
  local copies, waits for them, and re-layouts  12.8 us (5%)
  loops' own time  8.52 us (3%)
  starting transfers between devices  3.86 us (2%)
    reduce_scatter x1, waiting for transfers between devices, shards(): lax.psum_scatter((lax.dot_general(att_out_weight, att_mixed, contract, pr...  103 us
    all_gather x1, blocking collectives, shards(): lax.all_gather(key_rot, 'sp', axis=0, tiled=True)  44.6 us
    reduce_sum x1, other arithmetic, shards(): jnp.sum(conv_out, axis=1)  14.7 us
    all_gather x1, waiting for transfers between devices, shards(): lax.all_gather(tokens, 'tp', axis=1, tiled=True).astype(jnp.float32)  14.1 us
    dot_general x6, matrix products, add_product(): return jnp.dot(scaled, weight, preferred_element_type=jnp.float32)  9.11 us
    another operation x1, loops' own time, shards(): lax.scan(visit_block, start_state, jnp.arange(piece_rows // step_len, dty...  8.29 us
    dynamic_slice x12, local copies, waits for them, and re-layouts, shards(): lax.scan(visit_block, start_state, jnp.arange(piece_rows // step_len, dty...  7.04 us
  transfers between devices with their start and end apart: 4, of which 2 were waited for; matrix products, arithmetic and copies ran while one was open for 10% of the time, Pallas kernels for 0%

commit v1 on v0

--- a/solution.py
+++ b/solution.py
@@ -72,7 +72,7 @@
         conv_value_weight,
         conv_gate_weight,
     )
-    wide_part = lax.all_gather(tokens, "tp", axis=1, tiled=True).astype(jnp.float32)
+    wide_part = jnp.concatenate(lax.all_gather(tokens, "tp"), axis=1).astype(jnp.float32)
     scaled = (wide_part * input_gain[None, :]).astype(jnp.bfloat16)
 
     def add_product(weight):

time: 250 us -> 260 us (1.040)
  other arithmetic: 22.4 us -> 28 us
  local copies, waits for them, and re-layouts: 12.8 us -> 18.3 us
    convert_element_type x0 -> x2, other arithmetic: none -> 5.74 us  [the longest x1 3.43 us: shards(): jnp.concatenate(lax.all_gather(tokens, 'tp'), axis=1).astype(jnp.float32)]
    convert_element_type x0 -> x1, local copies, waits for them, and re-layouts: none -> 3.56 us  [shards(): jnp.concatenate(lax.all_gather(tokens, 'tp'), axis=1).astype(jnp.float32)]
    unnamed x35 -> x39, local copies, waits for them, and re-layouts: 4.75 us -> 6.67 us
where the time goes in v1:
time: 260 us; the launch traced here: 258 us
  waiting for transfers between devices  117 us (45%)
  blocking collectives  50 us (19%)
  other arithmetic  28 us (11%)
  local copies, waits for them, and re-layouts  18.3 us (7%)
  matrix products  18.2 us (7%)
  between operations  13.5 us (5%)
  loops' own time  8.52 us (3%)
  starting transfers between devices  3.86 us (1%)
    reduce_scatter x1, waiting for transfers between devices, shards(): lax.psum_scatter((lax.dot_general(att_out_weight, att_mixed, contract, pr...  103 us
    all_gather x1, blocking collectives, shards(): lax.all_gather(key_rot, 'sp', axis=0, tiled=True)  44.8 us
    reduce_sum x1, other arithmetic, shards(): jnp.sum(conv_out, axis=1)  14.7 us
    all_gather x1, waiting for transfers between devices, shards(): lax.all_gather(tokens, 'tp')  14.1 us
    another operation x1, loops' own time, shards(): lax.scan(visit_block, start_state, jnp.arange(piece_rows // step_len, dty...  8.29 us
    dot_general x6, matrix products, add_product(): return jnp.dot(scaled, weight, preferred_element_type=jnp.float32)  7.21 us
    dynamic_slice x12, local copies, waits for them, and re-layouts, shards(): lax.scan(visit_block, start_state, jnp.arange(piece_rows // step_len, dty...  7.04 us
    unnamed x39, local copies, waits for them, and re-layouts  6.67 us
  transfers between devices with their start and end apart: 4, of which 2 were waited for; matrix products, arithmetic and copies ran while one was open for 10% of the time, Pallas kernels for 0%

profile of v1, /device:TPU:0, one launch (start us, length us, event | category | flops | bytes accessed | tf_op | source)
XLA Modules:
  0.0 257.9 jit_solution(12411284649723302253)
XLA Ops:
  7.3 14.1 %all-gather.6.cloned.1.call-done = bf16[768,1024]{1,0:T(8,128)(2,1)} async-done(((bf16[384,1024]{1,0:T(8,128)(2,1)}), bf16[768,1024]{1,0:T(8,128)(2,1)}) %all-gather.6.cloned.1.call-update) | async-done | bytes 1572880 | tf_op jit(solution)/shard_map/all_gather | solution.py:75
  21.4 3.4 %convert_bitcast_fusion = f32[384,2,1024]{2,0,1:T(8,128)} fusion(bf16[2,384,1024]{2,1,0:T(8,128)(2,1)} %bitcast.95), kind=kLoop, calls=%fused_computation.60 | loop fusion | flops 786432 | bytes 4718592 | tf_op jit(solution)/shard_map/convert_element_type | solution.py:75
  24.9 3.6 %copy.26 = f32[384,2,1024]{0,2,1:T(8,128)} copy(f32[384,2,1024]{2,0,1:T(8,128)} %convert_bitcast_fusion) | data formatting | bytes 6291456 | tf_op jit(solution)/shard_map/convert_element_type | solution.py:75
  28.4 2.3 fusion.27
  33.5 1.8 fusion.26
  35.4 3.3 %fusion.33 = f32[384,512]{1,0:T(8,128)S(1)} fusion(bf16[384,2048]{0,1:T(8,128)(2,1)} %copy-done.1, bf16[2048,512]{1,0:T(8,128)(2,1)} %param.32, f32[384]{0:T(512)S(1)} %add_rsqrt_fusion.3), kind=kOutput, calls=%fused_computation.73 | convolution fusion | flops 806092800 | bytes 4457984 | tf_op jit(solution)/shard_map/dot_general | solution.py:79
  39.8 3.8 %collective-permute-start = (bf16[30,512]{1,0:T(8,128)(2,1)S(1)}, bf16[30,512]{1,0:T(8,128)(2,1)S(1)}, u32[]{:S(2)}, u32[]{:S(2)}) collective-permute-start(bf16[30,512]{1,0:T(8,128)(2,1)S(1)} %slice.268), channel_id=1, source_target_pairs={{0,2},{2,4},{4,6},{6,8},{8,10},{10,12},{12,14},{14,16},{16,18},{18... | collective-permute-start | bytes 92168 | tf_op jit(solution)/shard_map/ppermute | solution.py:22
  44.1 44.8 %all_gather.15 = bf16[6144,32]{0,1:T(8,128)(2,1)} all-gather(bf16[384,32]{0,1:T(8,128)(2,1)S(1)} %pad_maximum_fusion.2), channel_id=1, replica_groups=mesh['sp'=16,'tp'=2] {'sp'}, dimensions={0}, use_global_device_ids=true | all-gather | bytes 417792 | tf_op jit(solution)/shard_map/all_gather | solution.py:152
  91.8 14.7 %fusion.70 = (f32[384]{0:T(512)}, f32[384]{0:T(512)}, f32[384,512]{1,0:T(8,128)S(1)}) fusion(bf16[384,512]{1,0:T(8,128)(2,1)} %copy-done.7, f32[512]{0:T(512)S(1)} %bitcast.109, bf16[30,512]{1,0:T(8,128)(2,1)S(1)} %collective-permute-done, f32[512]{0:T(512)S(1)} %bitcast.110, f32[512]{0:T(512)} %bitcast.112, f32[512]{0:T(512)} %bitcast.113, ...), kind=kLoop, calls=%fused_computation.145 | loop fusion | flops 36371712 | bytes 1276928 | tf_op jit(solution)/shard_map/reduce_sum | solution.py:187
  106.5 2.8 %all-reduce.1 = (f32[384]{0:T(512)S(1)}, f32[384]{0:T(512)S(1)}) all-reduce(f32[384]{0:T(512)} %get-tuple-element.284, f32[384]{0:T(512)} %get-tuple-element.283), channel_id=1, replica_groups=mesh['sp'=16,'tp'=2] {'tp'}, use_global_device_ids=true, to_apply=%region_13.14 | all-reduce | flops 768 | bytes 6144 | tf_op jit(solution)/shard_map/psum | solution.py:186
  109.3 1.2 multiply_reduce_fusion
  110.4 4.7 %copy.28 = bf16[6144,256]{1,0:T(8,128)(2,1)} copy(bf16[6144,256]{0,1:T(8,128)(2,1)} %all-gather.4.cloned.1.call-done) | data formatting | bytes 6291456
  115.2 24.4 %while.15 = (s32[]{:T(128)}, f32[8,384]{1,0:T(8,128)S(1)}, f32[8,384]{1,0:T(8,128)S(1)}, f32[384,8,64]{0,2,1:T(8,128)S(1)}, s32[12]{0:T(128)S(1)}, /*index=5*/s3...) while((s32[]{:T(128)}, f32[8,384]{1,0:T(8,128)S(1)}, ...), condition=%wide.region_7.8_spmd.clone, body=%wide.region_2.7_spmd.clone.sunk | while | flops 788604800 | bytes 38840728 | solution.py:169
  116.5 9.0 %conditional.3 = ((f32[8,384]{1,0:T(8,128)S(1)}, f32[8,384]{1,0:T(8,128)S(1)}, f32[384,8,64]{0,2,1:T(8,128)S(1)})) conditional(s32[]{:T(128)} %convert_element_type.321, (f32[8,384]{1,0:T(8,128)S(1)}, f32[8,384]{1,0:T(8,128)S(1)}, f32[384,8,64]{0,2,1:T(8,128)S(1)}) %tuple.86, (s32[]{:T(128)}, s32[]{:T(128)}, bf16[6144,256]{1,0:T(8,128)(2,1)}, ...), branch_computations={%region_3.3_spmd, %region_4.6_spmd} | conditional | flops 788604800 | bytes 38838896 | solution.py:167
  116.5 1.4 convolution_convert_fusion.1
  117.9 1.9 fusion.18
  120.0 1.6 select_reduce_fusion
  121.6 1.3 convolution_convert_fusion
  122.9 1.4 fusion.13
  124.3 1.1 fusion.4
  140.6 2.4 all-reduce
  143.1 1.3 fusion.37
  146.3 2.5 fusion.28
  148.7 102.6 %reduce-scatter.2.cloned.1.call-done = bf16[1024,384]{0,1:T(8,128)(2,1)} async-done(((bf16[2048,384]{0,1:T(8,128)(2,1)}), bf16[1024,384]{0,1:T(8,128)(2,1)}) %reduce-scatter.2.cloned.1.call-update) | async-done | bytes 786448 | tf_op jit(solution)/shard_map/reduce_scatter | solution.py:203
  (115 shorter events, 18.2 us)
Async XLA Ops:
  6.5 137.8 %copy-start = (bf16[512,2048]{1,0:T(8,128)(2,1)S(1)}, bf16[512,2048]{1,0:T(8,128)(2,1)}, u32[]{:S(2)}) copy-start(bf16[512,2048]{1,0:T(8,128)(2,1)} %param.38) | copy-start | bytes 6291460
  6.5 14.9 %all-gather.6.cloned.1.call-start = ((), (), s32[]{:S(2)}) async-start(), calls=%async_computation.3 | async-start | bytes 2359296 | tf_op jit(solution)/shard_map/all_gather | solution.py:75
  7.3 103.2 %all-gather.4.cloned.1.call-start = ((), (), s32[]{:S(2)}) async-start(), calls=%async_computation.1 | async-start | bytes 3342336 | tf_op jit(solution)/shard_map/all_gather | solution.py:151
  24.9 3.6 %copy-start.10 = (f32[2048]{0:T(1024)S(1)}, f32[2048]{0:T(1024)}, u32[]{:S(2)}) copy-start(f32[2048]{0:T(1024)} %param.23) | copy-start | bytes 24580
  28.4 2.3 copy-start.17
  30.8 1.2 copy-start.1
  30.8 1.2 copy-start.14
  30.8 2.0 copy-start.9
  32.7 218.6 %reduce-scatter.2.cloned.1.call-start = ((), (), s32[]{:S(2)}) async-start(), calls=%async_computation.2 | async-start | bytes 2359296 | tf_op jit(solution)/shard_map/reduce_scatter | solution.py:203
  35.3 3.4 %copy-start.2 = (bf16[384,2048]{0,1:T(8,128)(2,1)S(1)}, bf16[384,2048]{0,1:T(8,128)(2,1)}, u32[]{:S(2)}) copy-start(bf16[384,2048]{0,1:T(8,128)(2,1)} %copy-done.1) | copy-start | bytes 4718596
  35.4 3.4 %copy-start.6 = (bf16[2048,512]{1,0:T(8,128)(2,1)S(1)}, bf16[2048,512]{1,0:T(8,128)(2,1)}, u32[]{:S(2)}) copy-start(bf16[2048,512]{1,0:T(8,128)(2,1)} %param.31) | copy-start | bytes 6291460
  38.7 4.8 %copy-start.8 = (bf16[2048,32]{0,1:T(8,128)(2,1)S(1)}, bf16[2048,32]{0,1:T(8,128)(2,1)}, u32[]{:S(2)}) copy-start(bf16[2048,32]{0,1:T(8,128)(2,1)} %param.27) | copy-start | bytes 393220
  39.7 50.0 %copy-start.7 = (bf16[384,512]{1,0:T(8,128)(2,1)}, bf16[384,512]{1,0:T(8,128)(2,1)S(1)}, u32[]{:S(2)}) copy-start(bf16[384,512]{1,0:T(8,128)(2,1)S(1)} %fusion.35) | copy-start | bytes 1179652
  39.8 49.2 %copy-start.18 = (bf16[2048,256]{1,0:T(8,128)(2,1)S(1)}, bf16[2048,256]{1,0:T(8,128)(2,1)}, u32[]{:S(2)}) copy-start(bf16[2048,256]{1,0:T(8,128)(2,1)} %param.25) | copy-start | bytes 3145732
  39.8 52.0 %collective-permute-start = (bf16[30,512]{1,0:T(8,128)(2,1)S(1)}, bf16[30,512]{1,0:T(8,128)(2,1)S(1)}, u32[]{:S(2)}, u32[]{:S(2)}) collective-permute-start(bf16[30,512]{1,0:T(8,128)(2,1)S(1)} %slice.268), channel_id=1, source_target_pairs={{0,2},{2,4},{4,6},{6,8},{8,10},{10,12},{12,14},{14,16},{16,18},{18... | collective-permute-start | bytes 92168 | tf_op jit(solution)/shard_map/ppermute | solution.py:22
  89.0 1.6 copy-start.15
  106.5 8.6 %copy-start.4 = (f32[384,512]{1,0:T(8,128)}, f32[384,512]{1,0:T(8,128)S(1)}, u32[]{:S(2)}) copy-start(f32[384,512]{1,0:T(8,128)S(1)} %get-tuple-element.317) | copy-start | bytes 2359300
  115.2 27.9 %copy-start.11 = (f32[512]{0:T(512)S(1)}, f32[512]{0:T(512)}, u32[]{:S(2)}) copy-start(f32[512]{0:T(512)} %param.36) | copy-start | bytes 6148
  120.0 1.6 copy-start.3
  144.4 1.1 copy-start.5
  144.4 1.1 copy-start.12
  144.4 1.1 copy-start.13
  144.4 1.9 copy-start.16
  144.4 1.8 copy-start.19
Sparse Core Ops, SparseCore 0:
  8.9 12.5 all-gather.5
  32.9 70.0 all-gather.3
  148.9 102.4 reduce-scatter.1
